TPU v7x, 512 devices: a whole 4x4x16 slice. The times are simulated.
512 devices in a mesh: sp: 16 (over z), dp: 32 (over y, x, core).
Axes of the slice: x: 4, y: 4, z: 16, core: 2. Of those that a mesh axis runs over, the one named last changes fastest.
Arguments:
- normed: bfloat16 [32, 2048, 2048], P('dp', 'sp'), may hold values from -6 to 6
- values: bfloat16 [32, 2048, 2048], P('dp', 'sp'), may hold values from -6 to 6
- gate_in: bfloat16 [32, 2048, 2048], P('dp', 'sp'), may hold values from -6 to 6
- step_raw: bfloat16 [32, 2048, 32], P('dp', 'sp'), may hold values from -3.5 to 2.5
- upstream: bfloat16 [32, 2048, 2048], P('dp', 'sp'), may hold values from -6 to 6
- proj_pair: bfloat16 [2048, 512], P('dp'), may hold values from -0.03125 to 0.03125
- conv_value: float32 [4, 2048], replicated, may hold values from -3 to 3
- conv_pair: float32 [4, 512], replicated, may hold values from -3 to 3
- step_bias: float32 [32], replicated, may hold values from -1 to 1
- decay_log: float32 [32], replicated, may hold values from -12 to -2
- skip: float32 [32], replicated, may hold values from 0.5 to 1.5
Outputs:
- grad_normed: bfloat16 [32, 2048, 2048], P('dp', 'sp')
- grad_values: bfloat16 [32, 2048, 2048], P('dp', 'sp')
- grad_gate: bfloat16 [32, 2048, 2048], P('dp', 'sp')
- grad_step: bfloat16 [32, 2048, 32], P('dp', 'sp')
- grad_proj: float32 [2048, 512], P('dp')
All inputs are finite; a program needn't handle non-finite values.
Results may differ from a plain program's by a relative error of at most 0.02.
Values may be sent and summed in bfloat16 or wider, within the bound.
A program may use at most 128 MiB of HBM per device.

v0:
```python
import jax
import jax.numpy as jnp
from jax import lax
from jax.sharding import PartitionSpec as P

HEADS = 32
HEAD = 64
GROUPS = 2
STATE = 128
BLOCK = 64


exact = lax.Precision.HIGHEST


def from_everyone(x, axis):
    devices = lax.axis_size(axis)
    return lax.all_to_all(jnp.broadcast_to(x[None], (devices, *x.shape)), axis, 0, 0, tiled=True)


def in_order(blocks, dim):
    lengths = list(blocks.shape[1:])
    lengths[dim] *= blocks.shape[0]
    return jnp.moveaxis(blocks, 0, dim).reshape(lengths)


def gathered_copies(x, axis, dim):
    blocks = from_everyone(x, axis)
    return in_order(blocks, dim)


def in_one_piece(arrays, axis, split_dim, concat_dim, along):
    both = jnp.concatenate(arrays, axis=along)
    whole, at, finished = (
        lax.all_to_all(both, axis, split_axis=split_dim, concat_axis=concat_dim, tiled=True),
        0,
        [],
    )
    for a in arrays:
        finished.append(lax.slice_in_dim(whole, at, at + a.shape[along], axis=along))
        at += a.shape[along]
    return tuple(finished)


def over_pieces(x, axis):
    blocks = lax.all_gather(x, axis).astype(jnp.float32)
    return blocks.sum(axis=0)


def causal_filter(signal, weights):
    length = signal.shape[0]
    tap_count = weights.shape[0]
    padded = jnp.pad(signal, ((tap_count - 1, 0), (0, 0)))
    summed = jnp.zeros_like(signal)
    for offset in range(tap_count):
        summed = summed + weights[offset] * padded[offset : offset + length]
    return jax.nn.silu(summed)


def silu_slope(gate):
    sig = jax.nn.sigmoid(gate)
    return sig * (1.0 + gate * (1.0 - sig))


def scan_heads(
    head_value, pair_rows, raw_steps, taps_value, taps_pair, biases, log_rates, skip_gains
):
    length, width = head_value.shape
    count = raw_steps.shape[1]
    head_dim = width // count
    state_dim = pair_rows.shape[1] // 2
    blocks = length // BLOCK
    conv_values = causal_filter(head_value, taps_value)
    conv_pairs = causal_filter(pair_rows, taps_pair)
    inject = conv_pairs[:, :state_dim].reshape(blocks, BLOCK, state_dim)
    readout = conv_pairs[:, state_dim:].reshape(blocks, BLOCK, state_dim)
    step_size = jax.nn.softplus(raw_steps + biases[None, :])
    decay_rate = -jnp.exp(log_rates)
    within = jnp.cumsum((step_size * decay_rate[None, :]).reshape(blocks, BLOCK, count), axis=1)
    value_heads = conv_values.reshape(length, count, head_dim)
    scaled = (value_heads * step_size[:, :, None]).reshape(blocks, BLOCK, count, head_dim)
    causal = jnp.tril(jnp.ones((BLOCK, BLOCK), dtype=bool))
    intersect = jnp.einsum("cln,csn->cls", readout, inject, precision=exact)
    spacing = within[:, :, None, :] - within[:, None, :, :]
    weight_diag = jnp.exp(jnp.where(causal[None, :, :, None], spacing, -jnp.inf))
    mixing = intersect[:, :, :, None] * weight_diag
    local_out = jnp.einsum("clsh,cshp->clhp", mixing, scaled, precision=exact)
    to_end = jnp.exp(within[:, -1:, :] - within)
    carried = jnp.einsum("cln,clhp->chpn", inject, scaled * to_end[:, :, :, None], precision=exact)
    block_total = within[:, -1, :]
    running = jnp.cumsum(block_total, axis=0)
    earlier = jnp.tril(jnp.ones((blocks, blocks), dtype=bool), -1)
    link = jnp.exp(
        jnp.where(
            earlier[:, :, None], (running - block_total)[:, None, :] - running[None, :, :], -jnp.inf
        )
    )
    entering = jnp.einsum("cdh,dhpn->chpn", link, carried, precision=exact)
    far_raw = jnp.einsum("cln,chpn->clhp", readout, entering, precision=exact)
    far_out = far_raw * jnp.exp(within)[:, :, :, None]
    direct = (value_heads * skip_gains[None, :, None]).reshape(length, width)
    return (local_out + far_out).reshape(length, width) + direct


def head_grads(
    head_value,
    pair_rows,
    raw_steps,
    taps_value,
    taps_pair,
    biases,
    log_rates,
    skip_gains,
    cotangent,
):

    def forward(vals, pairs, raws):
        return scan_heads(vals, pairs, raws, taps_value, taps_pair, biases, log_rates, skip_gains)

    output, pullback = jax.vjp(forward, head_value, pair_rows, raw_steps)
    return (output, pullback(cotangent))


def per_device(
    normed,
    values,
    gate_in,
    step_raw,
    upstream,
    proj_pair,
    conv_value,
    conv_pair,
    step_bias,
    decay_log,
    skip,
):
    sp_size = lax.axis_size("sp")
    sp_index = lax.axis_index("sp")
    token_rows = normed[0]
    tok_count = token_rows.shape[0]
    full_proj = gathered_copies(proj_pair, "dp", 0)
    pair_pre = jnp.dot(token_rows, full_proj, preferred_element_type=jnp.float32).astype(
        jnp.bfloat16
    )
    pair_width = 2 * STATE
    per_group = sp_size // GROUPS
    spread = jnp.repeat(pair_pre.reshape(1, tok_count, GROUPS, pair_width), per_group, axis=2)
    spread = spread.reshape(1, tok_count, sp_size * pair_width)
    gate_float = gate_in.astype(jnp.float32)
    up_float = upstream.astype(jnp.float32)
    slim_cot = (up_float * jax.nn.silu(gate_float)).astype(jnp.bfloat16)
    head_vals, head_cot, head_raw, head_pairs = (
        *in_one_piece((values, slim_cot), "sp", 2, 1, 0),
        lax.all_to_all(step_raw, "sp", split_axis=2, concat_axis=1, tiled=True),
        lax.all_to_all(spread, "sp", split_axis=2, concat_axis=1, tiled=True),
    )
    heads_dev = head_raw.shape[2]
    width_dev = heads_dev * HEAD
    first_head = sp_index * heads_dev
    group = first_head // (HEADS // GROUPS)
    taps_value = lax.dynamic_slice_in_dim(conv_value, first_head * HEAD, width_dev, 1)
    taps_pair = lax.dynamic_slice_in_dim(conv_pair, group * pair_width, pair_width, 1)
    biases = lax.dynamic_slice_in_dim(step_bias, first_head, heads_dev, 0)
    log_rates = lax.dynamic_slice_in_dim(decay_log, first_head, heads_dev, 0)
    skip_gains = lax.dynamic_slice_in_dim(skip, first_head, heads_dev, 0)
    pair_float = head_pairs[0].astype(jnp.float32)
    head_value = head_vals[0].astype(jnp.float32)
    head_step = head_raw[0].astype(jnp.float32)
    cotangent = head_cot[0].astype(jnp.float32)
    output, grads = head_grads(
        head_value,
        pair_float,
        head_step,
        taps_value,
        taps_pair,
        biases,
        log_rates,
        skip_gains,
        cotangent,
    )
    out_round = output.astype(jnp.bfloat16)
    side_block = out_round[None]
    grad_block = grads[0].astype(jnp.bfloat16)[None]
    step_block = grads[2].astype(jnp.bfloat16)[None]
    pair_part = grads[1].astype(jnp.bfloat16)[None]
    tok_values, tok_side, tok_step, tok_pairs = (
        *in_one_piece((grad_block, side_block), "sp", 1, 2, 0),
        lax.all_to_all(step_block, "sp", split_axis=1, concat_axis=2, tiled=True),
        lax.all_to_all(pair_part, "sp", split_axis=1, concat_axis=2, tiled=True),
    )
    grad_gate = (up_float * tok_side.astype(jnp.float32) * silu_slope(gate_float)).astype(
        jnp.bfloat16
    )
    pair_sum = (
        tok_pairs[0]
        .astype(jnp.float32)
        .reshape(tok_count, GROUPS, per_group, pair_width)
        .sum(axis=2)
    )
    pair_total = pair_sum.reshape(tok_count, GROUPS * pair_width).astype(jnp.bfloat16)
    grad_normed = lax.dot_general(
        pair_total, full_proj, (((1,), (1,)), ((), ())), preferred_element_type=jnp.float32
    ).astype(jnp.bfloat16)[None]
    grad_rows = lax.psum_scatter(
        lax.dot_general(
            token_rows, pair_total, (((0,), (0,)), ((), ())), preferred_element_type=jnp.float32
        ).astype(jnp.bfloat16),
        "dp",
        scatter_dimension=0,
        tiled=True,
    )
    grad_proj = over_pieces(grad_rows, "sp").astype(jnp.float32)
    return (grad_normed, tok_values, grad_gate, tok_step, grad_proj)


def solution(mesh):
    in_specs = (
        P("dp", "sp", None),
        P("dp", "sp", None),
        P("dp", "sp", None),
        P("dp", "sp", None),
        P("dp", "sp", None),
        P("dp", None),
        P(),
        P(),
        P(),
        P(),
        P(),
    )
    out_specs = (
        P("dp", "sp", None),
        P("dp", "sp", None),
        P("dp", "sp", None),
        P("dp", "sp", None),
        P("dp", None),
    )
    return jax.shard_map(
        per_device, mesh=mesh, in_specs=in_specs, out_specs=out_specs, check_vma=False
    )
```

profile of v0, /device:TPU:6, one launch (start us, length us, event | category | flops | bytes accessed | tf_op | source)
XLA Modules:
  0.0 560.9 jit_solution(8682605007620674141)
XLA Ops:
  8.0 27.5 %all_to_all.86 = bf16[16,2,128]{2,1,0:T(2,128)(2,1)S(1)} all-to-all(bf16[16,2,128]{2,1,0:T(2,128)(2,1)S(1)} %bitcast.260), channel_id=1, replica_groups=mesh['sp'=16,'dp'=32] {'sp'}, dimensions={0} | all-to-all | bytes 16384 | tf_op jit(solution)/shard_map/all_to_all | solution.py:154
  35.4 2.4 broadcast_in_dim.80
  37.8 7.6 %all-to-all-start.2 = ((bf16[32,64,512]{2,1,0:T(8,128)(2,1)}), bf16[32,64,512]{2,1,0:T(8,128)(2,1)S(1)}, u32[]{:S(2)}, u32[]{:S(2)}) async-start(bf16[32,64,512]{2,1,0:T(8,128)(2,1)} %broadcast_in_dim.80), calls=%async_computation.2 | async-start | bytes 4194304 | tf_op jit(solution)/shard_map/all_to_all | solution.py:18
  53.3 9.5 %copy.307 = bf16[2,128,2048]{1,0,2:T(2,128)(2,1)} copy(bf16[2,128,2048]{1,2,0:T(8,128)(2,1)S(1)} %pad_maximum_fusion) | data formatting | bytes 2097152 | tf_op jit(solution)/shard_map/concatenate | solution.py:33
  62.8 8.1 %all-to-all-done.2 = bf16[32,64,512]{2,1,0:T(8,128)(2,1)S(1)} async-done(((bf16[32,64,512]{2,1,0:T(8,128)(2,1)}), bf16[32,64,512]{2,1,0:T(8,128)(2,1)S(1)}, u32[]{:S(2)}, u32[]{:S(2)}) %all-to-all-start.2) | async-done | bytes 2097184 | tf_op jit(solution)/shard_map/all_to_all | solution.py:18
  70.8 4.6 all-to-all-start
  76.2 16.7 %copy.480 = bf16[1,128,4096]{1,0,2:T(2,128)(2,1)S(1)} copy(bf16[1,128,4096]{1,2,0:T(8,128)(2,1)S(1)} %bitcast.241) | data formatting | bytes 2097152 | tf_op jit(solution)/shard_map/broadcast_in_dim | solution.py:147
  93.6 23.4 %reduce.1 = bf16[4096,128]{1,0:T(8,128)(2,1)} reduce(bf16[4096,1,128]{2,1,0:T(2,128)(2,1)S(1)} %bitcast.235, bf16[]{:T(256)} %broadcast.179), dimensions={1}, to_apply=%bitcast.219.reduce_sub_computation | reduce | bytes 2097154
  117.0 2.2 reshape.403
  119.2 2.3 all-to-all-done
  121.5 13.3 %all-to-all-start.3 = ((bf16[16,2,16384]{2,1,0:T(2,128)(2,1)}), bf16[16,2,16384]{2,1,0:T(2,128)(2,1)}, u32[]{:S(2)}, u32[]{:S(2)}) async-start(bf16[16,2,16384]{2,1,0:T(2,128)(2,1)} %reshape.403), calls=%async_computation.3 | async-start | bytes 2097152 | tf_op jit(solution)/shard_map/all_to_all | solution.py:155
  138.0 6.6 %fusion.143 = f32[32,64,2]{2,0,1:T(8,128)S(1)} fusion(f32[32,64,2]{2,0,1:T(8,128)S(1)} %copy.313), kind=kOutput, calls=%fused_computation.195 | output fusion | flops 258048 | bytes 32768 | tf_op jit(solution)/shard_map/jvp(jit(cumsum))/reduce_window_sum | solution.py:79
  151.5 4.1 fusion.107
  156.9 2.5 reshape.398
  164.2 2.7 copy.319
  167.0 18.1 %all-to-all-done.3 = bf16[16,2,16384]{2,1,0:T(2,128)(2,1)} async-done(((bf16[16,2,16384]{2,1,0:T(2,128)(2,1)}), bf16[16,2,16384]{2,1,0:T(2,128)(2,1)}, u32[]{:S(2)}, u32[]{:S(2)}) %all-to-all-start.3) | async-done | bytes 1048608 | tf_op jit(solution)/shard_map/all_to_all | solution.py:155
  185.1 5.8 %reshape.404 = bf16[4096,1,128]{2,1,0:T(2,128)(2,1)} reshape(bf16[16,2,16384]{2,1,0:T(2,128)(2,1)} %all-to-all-done.3) | data formatting | bytes 2097152
  194.2 3.3 copy.326
  197.5 6.2 %fusion.16 = (f32[2048,256]{1,0:T(8,128)S(1)}, f32[2048,256]{1,0:T(8,128)}) fusion(f32[2048,256]{1,0:T(8,128)} %bitcast.237, f32[256]{0:T(256)S(1)} %bitcast.268, f32[256]{0:T(256)S(1)} %bitcast.266, f32[256]{0:T(256)S(1)} %bitcast.264, f32[256]{0:T(256)S(1)} %bitcast.262), kind=kLoop, calls=%fused_computation.31 | loop fusion | flops 5767168 | bytes 6295552 | tf_op jit(solution)/shard_map/jvp(jit(silu))/mul | solution.py:57
  205.3 2.4 fusion.41
  207.7 3.3 fusion.38
  211.0 4.5 multiply_reduce_fusion
  216.4 6.3 %fusion.53 = f32[32,64,128]{2,1,0:T(8,128)S(1)} fusion(f32[32,2,64,128]{3,0,2,1:T(8,128)} %copy-done.13, f32[32,64,2,64]{1,3,2,0:T(8,128)S(1)} %copy.319, f32[32,64,2]{1,2,0:T(2,128)S(1)} %copy.322, f32[32,64,2]{1,2,0:T(2,128)S(1)} %copy.318), kind=kOutput, calls=%fused_computation.64 | convolution fusion | flops 403177472 | bytes 4227072 | tf_op jit(solution)/shard_map/transpose(jvp(cln,clhp->chpn))/dot_general | solution.py:89
  222.8 2.2 fusion.33
  225.0 4.6 fusion.138
  229.6 3.5 fusion.35
  233.2 4.7 fusion.58
  239.8 3.7 fusion.62
  249.1 13.0 %copy.479 = bf16[1,2048,256]{2,0,1:T(2,128)(2,1)} copy(bf16[1,2048,256]{2,1,0:T(8,128)(2,1)S(1)} %fusion.88) | data formatting | bytes 2097152 | tf_op jit(solution)/shard_map/broadcast_in_dim | solution.py:185
  262.1 12.7 %reduce.2 = bf16[2048,256]{1,0:T(8,128)(2,1)} reduce(bf16[2048,1,256]{2,1,0:T(2,128)(2,1)} %bitcast.236, bf16[]{:T(256)} %broadcast.179), dimensions={1}, to_apply=%bitcast.218.reduce_sub_computation | reduce | bytes 2097154
  276.9 8.2 %all-to-all-start.4 = ((bf16[16,2,16384]{2,1,0:T(2,128)(2,1)}), bf16[16,2,16384]{2,1,0:T(2,128)(2,1)}, u32[]{:S(2)}, u32[]{:S(2)}) async-start(bf16[16,2,16384]{2,1,0:T(2,128)(2,1)} %reshape.407), calls=%async_computation.4 | async-start | bytes 2097152 | tf_op jit(solution)/shard_map/all_to_all | solution.py:189
  285.1 5.6 bitcast_add_fusion.1
  291.3 4.1 copy.397
  295.4 4.2 copy.347
  302.7 5.7 %fusion.4 = (f32[32,64,2]{1,2,0:T(2,128)S(1)}, f32[32,64,2,64]{1,3,2,0:T(8,128)S(1)}) fusion(bf16[32,64,2,64]{1,0,3,2:T(8,128)(2,1)} %copy-done.1, f32[32,64,128,1]{2,1,3,0:T(8,128)} %bitcast.228, f32[32,2,64,128]{3,0,2,1:T(8,128)} %copy-done.8), kind=kOutput, calls=%fused_computation.9 | convolution fusion | flops 403435520 | bytes 4734976 | tf_op jit(solution)/shard_map/jvp(cln,chpn->clhp)/dot_general | solution.py:99
  308.4 5.2 bitcast_add_fusion
  313.6 3.1 copy.398
  324.6 3.3 reshape.399
  333.5 13.6 %reduce.3 = bf16[2048,2]{1,0:T(8,128)(2,1)} reduce(bf16[2048,1,2]{2,1,0:T(2,128)(2,1)} %bitcast.245, bf16[]{:T(256)} %broadcast.179), dimensions={1}, to_apply=%bitcast.190.reduce_sub_computation | reduce | bytes 16386
  347.2 2.2 reshape.409
  349.4 3.3 broadcast_multiply_fusion.4
  354.1 12.1 %all-to-all-start.6 = ((bf16[16,2,128]{2,1,0:T(2,128)(2,1)}), bf16[16,2,128]{2,1,0:T(2,128)(2,1)S(1)}, u32[]{:S(2)}, u32[]{:S(2)}) async-start(bf16[16,2,128]{2,1,0:T(2,128)(2,1)} %reshape.409), calls=%async_computation.6 | async-start | bytes 16384 | tf_op jit(solution)/shard_map/all_to_all | solution.py:188
  366.3 4.3 reshape.408
  373.9 2.5 copy.399
  377.7 9.5 %copy.353 = bf16[2,2048,128]{2,0,1:T(2,128)(2,1)} copy(bf16[2,2048,128]{2,1,0:T(8,128)(2,1)S(1)} %pad_maximum_fusion.1) | data formatting | bytes 2097152 | tf_op jit(solution)/shard_map/concatenate | solution.py:33
  387.2 12.0 %all-to-all-start.5 = ((bf16[2,2048,128]{2,0,1:T(2,128)(2,1)}), bf16[2,2048,128]{2,0,1:T(2,128)(2,1)S(1)}, u32[]{:S(2)}, u32[]{:S(2)}) async-start(bf16[2,2048,128]{2,0,1:T(2,128)(2,1)} %copy.353), calls=%async_computation.5 | async-start | bytes 2097152 | tf_op jit(solution)/shard_map/all_to_all | solution.py:35
  399.3 79.8 %reduce-scatter.4.cloned.1.call-done = bf16[64,512]{1,0:T(8,128)(2,1)} async-done(((bf16[2048,512]{1,0:T(8,128)(2,1)}), bf16[64,512]{1,0:T(8,128)(2,1)}) %reduce-scatter.4.cloned.1.call-update) | async-done | bytes 65552 | tf_op jit(solution)/shard_map/reduce_scatter | solution.py:204
  491.9 59.7 %all-gather.3.cloned.1.call-done = bf16[1024,512]{1,0:T(8,128)(2,1)} async-done(((bf16[64,512]{1,0:T(8,128)(2,1)}), bf16[1024,512]{1,0:T(8,128)(2,1)}) %all-gather.3.cloned.1.call-update) | async-done | bytes 1048592 | tf_op jit(solution)/shard_map/all_gather | solution.py:46
  (209 shorter events, 79.2 us)
Async XLA Ops:
  7.2 68.2 %copy-start = (bf16[1,128,2048]{2,1,0:T(8,128)(2,1)S(1)}, bf16[1,128,2048]{2,1,0:T(8,128)(2,1)}, u32[]{:S(2)}) copy-start(bf16[1,128,2048]{2,1,0:T(8,128)(2,1)} %param.11) | copy-start | bytes 1572868
  37.8 33.0 %all-to-all-start.2 = ((bf16[32,64,512]{2,1,0:T(8,128)(2,1)}), bf16[32,64,512]{2,1,0:T(8,128)(2,1)S(1)}, u32[]{:S(2)}, u32[]{:S(2)}) async-start(bf16[32,64,512]{2,1,0:T(8,128)(2,1)} %broadcast_in_dim.80), calls=%async_computation.2 | async-start | bytes 4194304 | tf_op jit(solution)/shard_map/all_to_all | solution.py:18
  70.8 5.0 copy-start.9
  70.8 50.7 %all-to-all-start = ((bf16[2,128,2048]{1,0,2:T(2,128)(2,1)}), bf16[2,128,2048]{1,0,2:T(2,128)(2,1)}, u32[]{:S(2)}, u32[]{:S(2)}) async-start(bf16[2,128,2048]{1,0,2:T(2,128)(2,1)} %copy.307), calls=%async_computation | async-start | bytes 2097152 | tf_op jit(solution)/shard_map/all_to_all | solution.py:35
  117.0 17.9 %copy-start.48 = (f32[32]{0:T(128)S(1)}, f32[32]{0:T(128)}, u32[]{:S(2)}) copy-start(f32[32]{0:T(128)} %param.19) | copy-start | bytes 388
  117.0 18.0 %copy-start.49 = (f32[32]{0:T(128)S(1)}, f32[32]{0:T(128)}, u32[]{:S(2)}) copy-start(f32[32]{0:T(128)} %param.21) | copy-start | bytes 388
  117.0 18.8 %copy-start.50 = (f32[32]{0:T(128)S(1)}, f32[32]{0:T(128)}, u32[]{:S(2)}) copy-start(f32[32]{0:T(128)} %param.20) | copy-start | bytes 388
  117.0 19.6 %copy-start.46 = (f32[4,512]{1,0:T(4,128)S(1)}, f32[4,512]{1,0:T(4,128)}, u32[]{:S(2)}) copy-start(f32[4,512]{1,0:T(4,128)} %param.18) | copy-start | bytes 24580
  121.5 63.6 %all-to-all-start.3 = ((bf16[16,2,16384]{2,1,0:T(2,128)(2,1)}), bf16[16,2,16384]{2,1,0:T(2,128)(2,1)}, u32[]{:S(2)}, u32[]{:S(2)}) async-start(bf16[16,2,16384]{2,1,0:T(2,128)(2,1)} %reshape.403), calls=%async_computation.3 | async-start | bytes 2097152 | tf_op jit(solution)/shard_map/all_to_all | solution.py:155
  135.0 11.1 %copy-start.32 = (f32[2]{0:T(128)}, f32[2]{0:T(128)S(1)}, u32[]{:S(2)}) copy-start(f32[2]{0:T(128)S(1)} %dynamic_slice.16) | copy-start | bytes 28
  135.9 9.4 %copy-start.44 = (f32[2]{0:T(128)}, f32[2]{0:T(128)S(1)}, u32[]{:S(2)}) copy-start(f32[2]{0:T(128)S(1)} %exponential_negate_fusion) | copy-start | bytes 28
  136.7 60.8 %copy-start.28 = (f32[1,256]{1,0:T(1,128)}, f32[1,256]{1,0:T(1,128)S(1)}, u32[]{:S(2)}) copy-start(f32[1,256]{1,0:T(1,128)S(1)} %get-tuple-element.61) | copy-start | bytes 3076
  136.7 148.4 %copy-start.25 = (pred[64,64]{1,0:T(8,128)(4,1)}, pred[64,64]{1,0:T(8,128)(4,1)S(1)}, u32[]{:S(2)}) copy-start(pred[64,64]{1,0:T(8,128)(4,1)S(1)} %iota_compare_fusion) | copy-start | bytes 12292
  136.7 14.7 %copy-start.34 = (f32[128]{0:T(128)}, f32[128]{0:T(128)S(1)}, u32[]{:S(2)}) copy-start(f32[128]{0:T(128)S(1)} %get-tuple-element.63) | copy-start | bytes 1540
  136.7 14.7 %copy-start.36 = (f32[128]{0:T(128)}, f32[128]{0:T(128)S(1)}, u32[]{:S(2)}) copy-start(f32[128]{0:T(128)S(1)} %get-tuple-element.65) | copy-start | bytes 1540
  136.7 14.7 %copy-start.38 = (f32[128]{0:T(128)}, f32[128]{0:T(128)S(1)}, u32[]{:S(2)}) copy-start(f32[128]{0:T(128)S(1)} %get-tuple-element.66) | copy-start | bytes 1540
  136.8 14.7 %copy-start.40 = (f32[128]{0:T(128)}, f32[128]{0:T(128)S(1)}, u32[]{:S(2)}) copy-start(f32[128]{0:T(128)S(1)} %get-tuple-element.64) | copy-start | bytes 1540
  203.8 3.8 copy-start.6
  203.9 7.2 %copy-start.4 = (f32[2048,128]{1,0:T(8,128)}, f32[2048,128]{1,0:T(8,128)S(1)}, u32[]{:S(2)}) copy-start(f32[2048,128]{1,0:T(8,128)S(1)} %get-tuple-element.45) | copy-start | bytes 3145732
  207.7 3.3 copy-start.11
  211.0 4.5 copy-start.13
  216.4 6.4 %copy-start.5 = (f32[2048,128]{1,0:T(8,128)S(1)}, f32[2048,128]{1,0:T(8,128)}, u32[]{:S(2)}) copy-start(f32[2048,128]{1,0:T(8,128)} %copy-done.4) | copy-start | bytes 3145732
  229.6 61.1 %copy-start.30 = (f32[32,2]{0,1:T(2,128)}, f32[32,2]{0,1:T(2,128)S(1)}, u32[]{:S(2)}) copy-start(f32[32,2]{0,1:T(2,128)S(1)} %get-tuple-element.29) | copy-start | bytes 772
  229.6 3.5 copy-start.3
  233.2 4.8 copy-start.8
  233.2 4.8 copy-start.7
  239.7 3.7 copy-start.14
  276.9 77.2 %all-to-all-start.4 = ((bf16[16,2,16384]{2,1,0:T(2,128)(2,1)}), bf16[16,2,16384]{2,1,0:T(2,128)(2,1)}, u32[]{:S(2)}, u32[]{:S(2)}) async-start(bf16[16,2,16384]{2,1,0:T(2,128)(2,1)} %reshape.407), calls=%async_computation.4 | async-start | bytes 2097152 | tf_op jit(solution)/shard_map/all_to_all | solution.py:189
  295.4 5.1 copy-start.27
  302.7 5.7 %copy-start.15 = (f32[32,64,64]{2,1,0:T(8,128)S(1)}, f32[32,64,64]{2,1,0:T(8,128)}, u32[]{:S(2)}) copy-start(f32[32,64,64]{2,1,0:T(8,128)} %copy-done.14) | copy-start | bytes 1572868
  302.7 5.7 %copy-start.26 = (pred[64,64]{1,0:T(8,128)(4,1)S(1)}, pred[64,64]{1,0:T(8,128)(4,1)}, u32[]{:S(2)}) copy-start(pred[64,64]{1,0:T(8,128)(4,1)} %copy-done.25) | copy-start | bytes 12292
  316.8 2.3 copy-start.42
  322.6 5.3 copy-start.16
  327.9 3.4 copy-start.33
  327.9 3.4 copy-start.45
  331.2 18.1 %copy-start.19 = (f32[2048,128]{1,0:T(8,128)S(1)}, f32[2048,128]{1,0:T(8,128)}, u32[]{:S(2)}) copy-start(f32[2048,128]{1,0:T(8,128)} %reshape.400) | copy-start | bytes 3145732
  331.2 18.1 %copy-start.20 = (f32[2048,128]{1,0:T(8,128)S(1)}, f32[2048,128]{1,0:T(8,128)}, u32[]{:S(2)}) copy-start(f32[2048,128]{1,0:T(8,128)} %reshape.399) | copy-start | bytes 3145732
  331.3 18.1 %copy-start.41 = (f32[128]{0:T(128)S(1)}, f32[128]{0:T(128)}, u32[]{:S(2)}) copy-start(f32[128]{0:T(128)} %copy-done.40) | copy-start | bytes 1540
  331.3 18.1 %copy-start.47 = (f32[128]{0:T(128)S(1)}, f32[128]{0:T(128)}, u32[]{:S(2)}) copy-start(f32[128]{0:T(128)} %mul.386) | copy-start | bytes 1540
  349.4 3.3 copy-start.35
  349.4 3.3 copy-start.37
  349.4 3.3 copy-start.39
  354.1 33.1 %all-to-all-start.6 = ((bf16[16,2,128]{2,1,0:T(2,128)(2,1)}), bf16[16,2,128]{2,1,0:T(2,128)(2,1)S(1)}, u32[]{:S(2)}, u32[]{:S(2)}) async-start(bf16[16,2,128]{2,1,0:T(2,128)(2,1)} %reshape.409), calls=%async_computation.6 | async-start | bytes 16384 | tf_op jit(solution)/shard_map/all_to_all | solution.py:188
  366.2 112.9 %reduce-scatter.4.cloned.1.call-start = ((), (), s32[]{:S(2)}) async-start(), calls=%async_computation.9 | async-start | bytes 2162688 | tf_op jit(solution)/shard_map/reduce_scatter | solution.py:204
  387.2 94.4 %all-to-all-start.5 = ((bf16[2,2048,128]{2,0,1:T(2,128)(2,1)}), bf16[2,2048,128]{2,0,1:T(2,128)(2,1)S(1)}, u32[]{:S(2)}, u32[]{:S(2)}) async-start(bf16[2,2048,128]{2,0,1:T(2,128)(2,1)} %copy.353), calls=%async_computation.5 | async-start | bytes 2097152 | tf_op jit(solution)/shard_map/all_to_all | solution.py:35
  399.2 152.4 %all-gather.3.cloned.1.call-start = ((), (), s32[]{:S(2)}) async-start(), calls=%async_computation.8 | async-start | bytes 1114112 | tf_op jit(solution)/shard_map/all_gather | solution.py:46
  481.7 2.8 copy-start.18
  485.8 4.5 copy-start.10
  (11 other events, 18.0 us)
Sparse Core Ops, SparseCore 0:
  376.6 102.4 reduce-scatter.3
  481.1 70.4 all-gather.2
where the time goes:
time: 568 us; the launch traced here: 561 us
  waiting for transfers between devices  168 us (30%)
  local copies, waits for them, and re-layouts  142 us (25%)
  other arithmetic  91.2 us (16%)
  matrix products  59.4 us (10%)
  starting transfers between devices  57.9 us (10%)
  blocking collectives  27.5 us (5%)
  between operations  15.4 us (3%)
    reduce_scatter x1, waiting for transfers between devices, per_device(): lax.psum_scatter(lax.dot_general(token_rows, pair_total, (((0,), (0,)), (...  79.8 us
    all_gather x1, waiting for transfers between devices, over_pieces(): blocks = lax.all_gather(x, axis).astype(jnp.float32)  59.7 us
    unnamed x3, other arithmetic  49.8 us
    unnamed x120, local copies, waits for them, and re-layouts  35.7 us
    all_to_all x1, blocking collectives, per_device(): lax.all_to_all(step_raw, 'sp', split_axis=2, concat_axis=1, tiled=True)  27.5 us
    concatenate x2, local copies, waits for them, and re-layouts, in_one_piece(): both = jnp.concatenate(arrays, axis=along)  18.9 us
    all_to_all x1, waiting for transfers between devices, per_device(): lax.all_to_all(spread, 'sp', split_axis=2, concat_axis=1, tiled=True)  18.1 us
    broadcast_in_dim x2, local copies, waits for them, and re-layouts, per_device(): jnp.repeat(pair_pre.reshape(1, tok_count, GROUPS, pair_width), per_group,...  16.9 us
  transfers between devices with their start and end apart: 8, of which 5 were waited for; matrix products, arithmetic and copies ran while one was open for 34% of the time, Pallas kernels for 0%

commit v1 on v0

v1 whole, which is shorter than its diff:
```python
import functools

import jax
import jax.numpy as jnp
from jax import lax
from jax.experimental import pallas as pl
from jax.experimental.pallas import tpu as pltpu
from jax.sharding import PartitionSpec as P

HEADS = 32
HEAD = 64
GROUPS = 2
STATE = 128
TOK = 128
PAIRS = 16
TAPS = 4
CHUNKS = 16
RATIO = 3
MESH = pl.DeviceIdType.MESH
f32 = jnp.float32
bf16 = jnp.bfloat16
VM = pl.BlockSpec(memory_space=pltpu.VMEM)
SM = pl.BlockSpec(memory_space=pltpu.SMEM)
ANY = pl.BlockSpec(memory_space=pl.ANY)


def dot(a, b, ca, cb, precision=None):
    return lax.dot_general(
        a, b, (((ca,), (cb,)), ((), ())), precision=precision, preferred_element_type=f32
    )


def sigmoid(v):
    return 1.0 / (1.0 + jnp.exp(-v))


def remote(src, dst, send, recv, where):
    return pltpu.make_async_remote_copy(
        src_ref=src, dst_ref=dst, send_sem=send, recv_sem=recv, device_id=where, device_id_type=MESH
    )


def meet(places):
    barrier = pltpu.get_barrier_semaphore()
    for where in places:
        pl.semaphore_signal(barrier, inc=1, device_id=where, device_id_type=MESH)
    pl.semaphore_wait(barrier, len(places))


def gather_kernel(chips, n_sp, proj, values, normed, full, halo, ss, rs, fs, fr, hs, hr):
    z, d = lax.axis_index("sp"), lax.axis_index("dp")
    m, c = d // 2, lax.rem(d, 2)
    partner = {"dp": 2 * m + 1 - c}
    after, before = {"sp": lax.rem(z + 1, n_sp)}, {"sp": lax.rem(z + n_sp - 1, n_sp)}
    others = [lax.rem(m + k, chips) for k in range(1, chips)]
    meet([{"dp": 2 * t + c} for t in others] + [partner, after, before])
    sends = []
    for i, ref in enumerate((values, normed)):
        sends.append(remote(ref.at[0, pl.ds(TOK - 16, 16), :], halo.at[i], hs.at[i], hr.at[i], after))
    sends.append(remote(proj, full.at[m, c], fs.at[m], fr.at[m], partner))
    for k, t in enumerate(others):
        sends.append(remote(proj, full.at[m, c], ss.at[k], rs.at[m], {"dp": 2 * t + c}))
    for copy in sends:
        copy.start()
    full[m, c] = proj[...]
    for k in range(1, chips):
        src = lax.rem(m + chips - k, chips)
        remote(proj, full.at[src, c], ss.at[0], rs.at[src], partner).wait_recv()
        copy = remote(full.at[src, c], full.at[src, c], fs.at[src], fr.at[src], partner)
        copy.start()
        sends.append(copy)
    for src in range(chips):
        remote(proj, full.at[src, 1 - c], ss.at[0], fr.at[src], partner).wait_recv()
    for i in range(2):
        remote(halo.at[i], halo.at[i], hs.at[i], hr.at[i], after).wait_recv()
    for copy in sends:
        copy.wait_send()


def gather(proj, values, normed, chips, n_sp):
    rows, cols = proj.shape
    dma = pltpu.SemaphoreType.DMA
    return pl.pallas_call(
        functools.partial(gather_kernel, chips, n_sp),
        out_shape=(
            jax.ShapeDtypeStruct((chips, 2, rows, cols), bf16),
            jax.ShapeDtypeStruct((2, 16, values.shape[2]), bf16),
        ),
        in_specs=[VM, ANY, ANY],
        out_specs=(VM, VM),
        scratch_shapes=[dma((chips,)), dma((chips,)), dma((chips,)), dma((chips,)), dma((2,)), dma((2,))],
        compiler_params=pltpu.CompilerParams(collective_id=0, has_side_effects=True),
        name="gather",
    )(proj, values, normed)


def steps(raw_ref, bias_ref, log_ref):
    v = raw_ref[0].astype(f32) + bias_ref[...]
    dt = jnp.maximum(v, 0.0) + jnp.log1p(jnp.exp(-jnp.abs(v)))
    rate = -jnp.exp(log_ref[...])
    a = dt * rate
    row = lax.broadcasted_iota(jnp.int32, (TOK, TOK), 0)
    col = lax.broadcasted_iota(jnp.int32, (TOK, TOK), 1)
    lower = (col <= row).astype(f32)
    acum = dot(lower, a, 1, 0, lax.Precision.HIGHEST)
    acum_t = dot(a, lower, 0, 1, lax.Precision.HIGHEST)
    return v, dt, rate, acum, acum_t


def column(mat, h):
    lane = lax.broadcasted_iota(jnp.int32, mat.shape, 1)
    return jnp.sum(jnp.where(lane == h, mat, 0.0), axis=1, keepdims=True)


def first_half(rows=TOK):
    return lax.broadcasted_iota(jnp.int32, (rows, 128), 1) < HEAD


def pair_columns(mat, j):
    return jnp.where(first_half(mat.shape[0]), column(mat, 2 * j), column(mat, 2 * j + 1))


def slab(j):
    return pl.ds(pl.multiple_of(j * 128, 128), 128)


def conv_slab(ext, taps, cs):
    total = taps[0:1, cs] * ext[13 : 13 + TOK, cs]
    for k in range(1, TAPS):
        total = total + taps[k : k + 1, cs] * ext[13 + k : 13 + k + TOK, cs]
    return total


def extended(ext, halo, main, z):
    ext[0:16, :] = jnp.where(z > 0, halo.astype(f32), 0.0)
    ext[16 : 16 + TOK, :] = main.astype(f32)


def local_kernel(
    z_ref, full, normed, values, gate, up, raw, halo, taps_v, taps_p, bias, logs,
    bc_out, slope_out, left_out, right_out, dec_out, yl_out, dxl_out, dg_out,
    vext, pext, at_ref,
):
    z = z_ref[0]
    proj = full[...]
    pext[16 : 16 + TOK, :] = dot(normed[0], proj, 1, 0).astype(bf16).astype(f32)
    before = dot(halo[1], proj, 1, 0).astype(bf16).astype(f32)
    pext[0:16, :] = jnp.where(z > 0, before, 0.0)
    extended(vext, halo[0], values[0], z)
    _, dt, _, acum, acum_t = steps(raw, bias, logs)
    at_ref[...] = acum_t
    dec_out[...] = jnp.exp(jnp.broadcast_to(acum_t[:, TOK - 1 : TOK], (HEADS, 128)))
    for q in range(4):
        cs = slice(q * 128, q * 128 + 128)
        p = conv_slab(pext, taps_p, cs)
        sig = sigmoid(p)
        bc_out[:, cs] = p * sig
        slope_out[:, cs] = sig * (1.0 + p * (1.0 - sig))
    row = lax.broadcasted_iota(jnp.int32, (TOK, TOK), 0)
    col = lax.broadcasted_iota(jnp.int32, (TOK, TOK), 1)
    causal = col <= row
    half = first_half()
    for g in range(GROUPS):
        inject = bc_out[:, 256 * g : 256 * g + 128].astype(bf16)
        readout = bc_out[:, 256 * g + 128 : 256 * g + 256].astype(bf16)
        cross = dot(readout, inject, 1, 1)
        dg_out[g] = jnp.zeros((TOK, TOK), f32)

        def body(i, carry, g=g, inject=inject, readout=readout, cross=cross):
            j = g * (PAIRS // GROUPS) + i
            cs = slab(j)
            x = conv_slab(vext, taps_v, cs)
            u = x * sigmoid(x)
            a0, a1 = column(acum, 2 * j), column(acum, 2 * j + 1)
            ac = jnp.where(half, a0, a1)
            end = ac[TOK - 1 : TOK, :]
            xd = u * pair_columns(dt, j)
            v = gate[0, :, cs].astype(f32)
            cot = (up[0, :, cs].astype(f32) * v * sigmoid(v)).astype(bf16)
            xde = (xd * jnp.exp(end - ac)).astype(bf16)
            dye = (cot.astype(f32) * jnp.exp(ac)).astype(bf16)
            left_out[cs, :] = dot(xde, inject, 0, 0)
            right_out[cs, :] = dot(dye, readout, 0, 0)
            zero = jnp.zeros((), bf16)
            xb = xd.astype(bf16)
            xd0, xd1 = jnp.where(half, xb, zero), jnp.where(half, zero, xb)
            dy0, dy1 = jnp.where(half, cot, zero), jnp.where(half, zero, cot)
            l0 = jnp.exp(jnp.where(causal, a0 - at_ref[pl.ds(2 * j, 1), :], -jnp.inf))
            l1 = jnp.exp(jnp.where(causal, a1 - at_ref[pl.ds(2 * j + 1, 1), :], -jnp.inf))
            w0, w1 = (cross * l0).astype(bf16), (cross * l1).astype(bf16)
            yl_out[:, cs] = dot(w0, xd0, 1, 0) + dot(w1, xd1, 1, 0)
            dxl_out[:, cs] = dot(w0, dy0, 0, 0) + dot(w1, dy1, 0, 0)
            dg_out[g] += dot(dy0, xb, 1, 1) * l0 + dot(dy1, xb, 1, 1) * l1
            return carry

        lax.fori_loop(0, PAIRS // GROUPS, body, 0)


def local(z, full, normed, values, gate, up, raw, halo, taps_v, taps_p, bias, logs):
    width = values.shape[2]
    s = jax.ShapeDtypeStruct
    return pl.pallas_call(
        local_kernel,
        out_shape=(
            s((TOK, 512), f32), s((TOK, 512), f32), s((width, STATE), f32), s((width, STATE), f32),
            s((HEADS, 128), f32), s((TOK, width), f32), s((TOK, width), f32), s((GROUPS, TOK, TOK), f32),
        ),
        in_specs=[SM] + [VM] * 11,
        out_specs=(VM,) * 8,
        scratch_shapes=[
            pltpu.VMEM((16 + TOK, width), f32), pltpu.VMEM((16 + TOK, 512), f32), pltpu.VMEM((HEADS, TOK), f32),
        ],
        name="local",
    )(z, full, normed, values, gate, up, raw, halo, taps_v, taps_p, bias, logs)


def chain_kernel(n_sp, left, right, dec, s_in, ds_out, f_out, b_out, fs, fr, bs, br):
    z = lax.axis_index("sp")
    after, before = {"sp": lax.rem(z + 1, n_sp)}, {"sp": lax.rem(z + n_sp - 1, n_sp)}
    meet([after, before])
    rows = HEADS * HEAD // CHUNKS
    heads = HEADS // CHUNKS

    @pl.when(z == 0)
    def _():
        s_in[...] = jnp.zeros_like(s_in)

    @pl.when(z == n_sp - 1)
    def _():
        ds_out[...] = jnp.zeros_like(ds_out)

    def part(k):
        return pl.ds(pl.multiple_of(k * rows, rows), rows)

    def step(k, got, mine, out, send, recv, has, gives, where):
        at = part(k)
        copy = remote(out.at[at, :], got.at[at, :], send.at[k], recv.at[k], where)

        @pl.when(has)
        def _():
            copy.wait_recv()

        for i in range(heads):
            hs = pl.ds(pl.multiple_of(k * rows + i * HEAD, HEAD), HEAD)
            new = dec[pl.ds(k * heads + i, 1), :] * got[hs, :].astype(f32) + mine[hs, :]
            out[hs, :] = new.astype(bf16)

        @pl.when(gives)
        def _():
            copy.start()

    def tick(t, carry):
        kf = t - z * RATIO
        kb = t - (n_sp - 1 - z) * RATIO

        @pl.when((kf >= 0) & (kf < CHUNKS))
        def _():
            step(kf, s_in, left, f_out, fs, fr, z > 0, z < n_sp - 1, after)

        @pl.when((kb >= 0) & (kb < CHUNKS))
        def _():
            step(kb, ds_out, right, b_out, bs, br, z < n_sp - 1, z > 0, before)

        return carry

    lax.fori_loop(0, (n_sp - 1) * RATIO + CHUNKS, tick, 0)

    def finish(k, carry):
        at = part(k)

        @pl.when(z < n_sp - 1)
        def _():
            remote(f_out.at[at, :], s_in.at[at, :], fs.at[k], fr.at[k], after).wait_send()

        @pl.when(z > 0)
        def _():
            remote(b_out.at[at, :], ds_out.at[at, :], bs.at[k], br.at[k], before).wait_send()

        return carry

    lax.fori_loop(0, CHUNKS, finish, 0)


def chain(left, right, dec, n_sp):
    shape = jax.ShapeDtypeStruct(left.shape, bf16)
    dma = pltpu.SemaphoreType.DMA
    return pl.pallas_call(
        functools.partial(chain_kernel, n_sp),
        out_shape=(shape, shape),
        in_specs=[VM] * 3,
        out_specs=(VM, VM),
        scratch_shapes=[pltpu.VMEM(left.shape, bf16), pltpu.VMEM(left.shape, bf16)] + [dma((CHUNKS,))] * 4,
        compiler_params=pltpu.CompilerParams(collective_id=1, has_side_effects=True),
        name="chain",
    )(left, right, dec)


def grads_kernel(
    z_ref, values, gate, up, raw, halo, taps_v, taps_p, bias, logs, skips,
    bc, slope, left, dec, s_in, ds_out, yl, dxl, dg,
    gv_out, gg_out, gs_out, gv_tail, gv_halo, dp_out, dp_halo, dp_tail, dp_before,
    vext, dxs, dps, dbc, da_ref, dd_ref,
):
    z = z_ref[0]
    extended(vext, halo[0], values[0], z)
    v_step, dt, rate, acum, _ = steps(raw, bias, logs)
    half = first_half()
    keep = z > 0
    da_ref[...] = jnp.zeros_like(da_ref)
    dd_ref[...] = jnp.zeros_like(dd_ref)
    dxs[0:16, :] = jnp.zeros((16, 128), f32)
    dxs[16 + TOK :, :] = jnp.zeros((8, 128), f32)
    dps[0:16, :] = jnp.zeros((16, 512), f32)
    dps[16 + TOK :, :] = jnp.zeros((8, 512), f32)
    head_lane = lax.broadcasted_iota(jnp.int32, (TOK, HEADS), 1)
    last = lax.broadcasted_iota(jnp.int32, (TOK, HEADS), 0) == TOK - 1
    for g in range(GROUPS):
        inject = bc[:, 256 * g : 256 * g + 128].astype(bf16)
        readout = bc[:, 256 * g + 128 : 256 * g + 256].astype(bf16)
        dgb = dg[g].astype(bf16)
        dbc[:, 256 * g : 256 * g + 128] = dot(dgb, readout, 0, 0)
        dbc[:, 256 * g + 128 : 256 * g + 256] = dot(dgb, inject, 1, 0)

        def body(i, carry, g=g, inject=inject, readout=readout):
            j = g * (PAIRS // GROUPS) + i
            cs = slab(j)
            x = conv_slab(vext, taps_v, cs)
            sig = sigmoid(x)
            u = x * sig
            ac = pair_columns(acum, j)
            ea, ee = jnp.exp(ac), jnp.exp(ac[TOK - 1 : TOK, :] - ac)
            dtc = pair_columns(dt, j)
            xd = u * dtc
            v = gate[0, :, cs].astype(f32)
            upv = up[0, :, cs].astype(f32)
            gsig = sigmoid(v)
            cot = (upv * v * gsig).astype(bf16).astype(f32)
            xde, dye = (xd * ee).astype(bf16), (cot * ea).astype(bf16)
            s, ds = s_in[cs, :], ds_out[cs, :]
            y = yl[:, cs] + ea * dot(readout, s, 1, 1)
            dxd = dxl[:, cs] + ee * dot(inject, ds, 1, 1)
            dbc[:, 256 * g + 128 : 256 * g + 256] += dot(dye, s, 1, 0)
            dbc[:, 256 * g : 256 * g + 128] += dot(xde, ds, 1, 0)
            d0, d1 = dec[pl.ds(2 * j, 1), :], dec[pl.ds(2 * j + 1, 1), :]
            lf, sf, df = left[cs, :], s.astype(f32), ds.astype(f32)
            e0 = jnp.sum((d0 * sf[:HEAD] + lf[:HEAD]) * df[:HEAD])
            e1 = jnp.sum((d1 * sf[HEAD:] + lf[HEAD:]) * df[HEAD:])
            pa = cot * y - xd * dxd
            pd = u * dxd
            is0, is1 = head_lane == 2 * j, head_lane == 2 * j + 1
            sum0 = jnp.sum(jnp.where(half, pa, 0.0), axis=1, keepdims=True)
            sum1 = jnp.sum(jnp.where(half, 0.0, pa), axis=1, keepdims=True)
            da_ref[...] += jnp.where(is0, sum0 + jnp.where(last, e0, 0.0), 0.0) + jnp.where(
                is1, sum1 + jnp.where(last, e1, 0.0), 0.0
            )
            sum0 = jnp.sum(jnp.where(half, pd, 0.0), axis=1, keepdims=True)
            sum1 = jnp.sum(jnp.where(half, 0.0, pd), axis=1, keepdims=True)
            dd_ref[...] += jnp.where(is0, sum0, 0.0) + jnp.where(is1, sum1, 0.0)
            sk = skips[0:1, cs]
            ybf = (y + sk * u).astype(bf16).astype(f32)
            gg_out[0, :, cs] = (upv * ybf * (gsig * (1.0 + v * (1.0 - gsig)))).astype(bf16)
            du = dtc * dxd + sk * cot
            dxs[16 : 16 + TOK, :] = du * (sig * (1.0 + x * (1.0 - sig)))
            dv = taps_v[0:1, cs] * dxs[3 : 3 + 16 + TOK, :]
            for k in range(1, TAPS):
                dv = dv + taps_v[k : k + 1, cs] * dxs[3 - k : 3 - k + 16 + TOK, :]
            gv_out[0, :, cs] = dv[16:].astype(bf16)
            gv_tail[:, cs] = dv[TOK:]
            gv_halo[:, cs] = jnp.where(keep, dv[0:16], 0.0)
            return carry

        lax.fori_loop(0, PAIRS // GROUPS, body, 0)
    row = lax.broadcasted_iota(jnp.int32, (TOK, TOK), 0)
    col = lax.broadcasted_iota(jnp.int32, (TOK, TOK), 1)
    da = dot((col >= row).astype(f32), da_ref[...], 1, 0, lax.Precision.HIGHEST)
    gs_out[0] = ((rate * da + dd_ref[...]) * sigmoid(v_step)).astype(bf16)
    for q in range(4):
        cs = slice(q * 128, q * 128 + 128)
        dps[16 : 16 + TOK, cs] = dbc[:, cs] * slope[:, cs]
        dp = taps_p[0:1, cs] * dps[3 : 3 + 16 + TOK, cs]
        for k in range(1, TAPS):
            dp = dp + taps_p[k : k + 1, cs] * dps[3 - k : 3 - k + 16 + TOK, cs]
        dp_out[:, cs] = dp[16:].astype(bf16)
        dp_tail[:, cs] = dp[TOK:]
        before = jnp.where(keep, dp[0:16], 0.0)
        dp_before[:, cs] = before
        dp_halo[:, cs] = before.astype(bf16)


def grads(z, values, gate, up, raw, halo, taps_v, taps_p, bias, logs, skips, *rest):
    width = values.shape[2]
    s = jax.ShapeDtypeStruct
    return pl.pallas_call(
        grads_kernel,
        out_shape=(
            s((1, TOK, width), bf16), s((1, TOK, width), bf16), s((1, TOK, HEADS), bf16),
            s((16, width), f32), s((16, width), f32),
            s((TOK, 512), bf16), s((16, 512), bf16), s((16, 512), f32), s((16, 512), f32),
        ),
        in_specs=[SM] + [VM] * 19,
        out_specs=(VM,) * 9,
        scratch_shapes=[
            pltpu.VMEM((16 + TOK, width), f32), pltpu.VMEM((24 + TOK, 128), f32),
            pltpu.VMEM((24 + TOK, 512), f32), pltpu.VMEM((TOK, 512), f32),
            pltpu.VMEM((TOK, HEADS), f32), pltpu.VMEM((TOK, HEADS), f32),
        ],
        name="grads",
    )(z, values, gate, up, raw, halo, taps_v, taps_p, bias, logs, skips, *rest)


def reduce_kernel(
    chips, n_sp, normed, halo, dp, dp_halo, gv_halo, dp_before,
    out, gv_after, dp_after,
    mine, theirs, both, planes, zs, zr, zb, zc,
    cs_, cr, ps, pr, as_, ar, bs, br, hs, hr,
):
    z, d = lax.axis_index("sp"), lax.axis_index("dp")
    m, c = d // 2, lax.rem(d, 2)
    partner = {"dp": 2 * m + 1 - c}
    before = {"sp": lax.rem(z + n_sp - 1, n_sp)}
    plane = [lax.rem(m + k, chips) for k in range(1, chips)]
    line = [lax.rem(z + k, n_sp) for k in range(1, n_sp)]
    meet([{"dp": 2 * t + c} for t in plane] + [partner] + [{"sp": t} for t in line])
    sends = [
        remote(gv_halo, gv_after, hs.at[0], hr.at[0], before),
        remote(dp_before, dp_after, hs.at[1], hr.at[1], before),
    ]
    for copy in sends:
        copy.start()
    order = plane + [m]
    for k, t in enumerate(order):
        at = slab(t)
        block = dot(normed[0, :, at], dp[...], 0, 0) + dot(halo[1, :, at], dp_halo[...], 0, 0)
        mine[t] = block.astype(bf16).reshape(mine.shape[1:])
        copy = remote(mine.at[t, 1 - c], theirs.at[t], cs_.at[k], cr.at[t], partner)
        copy.start()
        sends.append(copy)
    for k, t in enumerate(order):
        remote(mine.at[t, 0], theirs.at[t], cs_.at[k], cr.at[t], partner).wait_recv()
        both[t] = (mine[t, c].astype(f32) + theirs[t].astype(f32)).astype(bf16)
        if k < chips - 1:
            copy = remote(both.at[t], planes.at[m], ps.at[k], pr.at[m], {"dp": 2 * t + c})
            copy.start()
            sends.append(copy)
    total = both[m].astype(f32)
    for k in range(1, chips):
        t = lax.rem(m + chips - k, chips)
        remote(both.at[t], planes.at[t], ps.at[0], pr.at[t], partner).wait_recv()
        total = total + planes[t].astype(f32)
    per = 16 // n_sp
    for q in range(16):
        tile = total[16 * (q // 4) : 16 * (q // 4) + 16, 128 * (q % 4) : 128 * (q % 4) + 128]
        zs[q // per, 16 * (q % per) : 16 * (q % per) + 16, :] = tile.astype(bf16)
    for k, t in enumerate(line):
        copy = remote(zs.at[t], zr.at[z], as_.at[k], ar.at[z], {"sp": t})
        copy.start()
        sends.append(copy)
    total = zs[z].astype(f32)
    for k in range(1, n_sp):
        t = lax.rem(z + n_sp - k, n_sp)
        remote(zs.at[t], zr.at[t], as_.at[0], ar.at[t], before).wait_recv()
        total = total + zr[t].astype(f32)
    zb[...] = total.astype(bf16)
    for k, t in enumerate(line):
        copy = remote(zb, zc.at[z], bs.at[k], br.at[z], {"sp": t})
        copy.start()
        sends.append(copy)
    zc[z] = zb[...]
    for k in range(1, n_sp):
        t = lax.rem(z + n_sp - k, n_sp)
        remote(zb, zc.at[t], bs.at[0], br.at[t], before).wait_recv()
    for q in range(16):
        tile = zc[q // per, 16 * (q % per) : 16 * (q % per) + 16, :].astype(f32)
        out[16 * (q // 4) : 16 * (q // 4) + 16, 128 * (q % 4) : 128 * (q % 4) + 128] = tile
    sends[0].wait_recv()
    sends[1].wait_recv()
    for copy in sends:
        copy.wait_send()


def reduce(normed, halo, dp, dp_halo, gv_halo, dp_before, chips, n_sp):
    dma = pltpu.SemaphoreType.DMA
    s = jax.ShapeDtypeStruct
    per = 16 // n_sp * 16
    return pl.pallas_call(
        functools.partial(reduce_kernel, chips, n_sp),
        out_shape=(s((64, 512), f32), s(gv_halo.shape, f32), s(dp_before.shape, f32)),
        in_specs=[VM] * 6,
        out_specs=(VM,) * 3,
        scratch_shapes=[
            pltpu.VMEM((chips, 2, 64, 512), bf16), pltpu.VMEM((chips, 64, 512), bf16),
            pltpu.VMEM((chips, 64, 512), bf16), pltpu.VMEM((chips, 64, 512), bf16),
            pltpu.VMEM((n_sp, per, 128), bf16), pltpu.VMEM((n_sp, per, 128), bf16),
            pltpu.VMEM((per, 128), bf16), pltpu.VMEM((n_sp, per, 128), bf16),
            dma((chips,)), dma((chips,)), dma((chips,)), dma((chips,)),
            dma((n_sp,)), dma((n_sp,)), dma((n_sp,)), dma((n_sp,)), dma((2,)), dma((2,)),
        ],
        compiler_params=pltpu.CompilerParams(collective_id=2, has_side_effects=True),
        name="reduce",
    )(normed, halo, dp, dp_halo, gv_halo, dp_before)


def finish_kernel(full, dp, dp_tail, dp_after, gv_tail, gv_after, gv_in, gn_out, gv_out):
    end = (dp_tail[...] + dp_after[...]).astype(bf16)
    dpair = jnp.concatenate([dp[0 : TOK - 16, :], end], axis=0)
    for q in range(full.shape[0] // 256):
        gn_out[0, :, 256 * q : 256 * q + 256] = dot(dpair, full[256 * q : 256 * q + 256, :], 1, 1).astype(bf16)
    gv_out[0] = (gv_tail[...] + gv_after[...]).astype(bf16)


def finish(full, dp, dp_tail, dp_after, gv_tail, gv_after, gv):
    s = jax.ShapeDtypeStruct
    whole = lambda a: pl.BlockSpec(a.shape, lambda i: (0,) * a.ndim)
    return pl.pallas_call(
        finish_kernel,
        grid=(1,),
        out_shape=(s((1, TOK, full.shape[0]), bf16), s(gv.shape, bf16)),
        in_specs=[whole(a) for a in (full, dp, dp_tail, dp_after, gv_tail, gv_after)] + [ANY],
        out_specs=(
            pl.BlockSpec((1, TOK, full.shape[0]), lambda i: (0, 0, 0)),
            pl.BlockSpec((1, 16, gv.shape[2]), lambda i: (0, TOK // 16 - 1, 0)),
        ),
        input_output_aliases={6: 1},
        name="finish",
    )(full, dp, dp_tail, dp_after, gv_tail, gv_after, gv)


def per_device(
    n_sp, n_dp, normed, values, gate_in, step_raw, upstream, proj_pair,
    conv_value, conv_pair, step_bias, decay_log, skip,
):
    z = lax.axis_index("sp").astype(jnp.int32).reshape(1)
    bias, logs = step_bias.reshape(1, HEADS), decay_log.reshape(1, HEADS)
    skips = jnp.repeat(skip, HEAD).reshape(1, HEADS * HEAD)
    chips = n_dp // 2
    full, halo = gather(proj_pair, values, normed, chips, n_sp)
    full = full.reshape(-1, full.shape[-1])
    bc, slope, left, right, dec, yl, dxl, dg = local(
        z, full, normed, values, gate_in, upstream, step_raw, halo, conv_value, conv_pair, bias, logs
    )
    s_in, ds_out = chain(left, right, dec, n_sp)
    gv, gg, gs, gv_tail, gv_halo, dp, dp_halo, dp_tail, dp_before = grads(
        z, values, gate_in, upstream, step_raw, halo, conv_value, conv_pair, bias, logs, skips,
        bc, slope, left, dec, s_in, ds_out, yl, dxl, dg,
    )
    gp, gv_after, dp_after = reduce(normed, halo, dp, dp_halo, gv_halo, dp_before, chips, n_sp)
    gn, gv = finish(full, dp, dp_tail, dp_after, gv_tail, gv_after, gv)
    return gn, gv, gg, gs, gp


def solution(mesh):
    tokens = P("dp", "sp", None)
    return jax.shard_map(
        functools.partial(per_device, mesh.shape["sp"], mesh.shape["dp"]),
        mesh=mesh,
        in_specs=(tokens,) * 5 + (P("dp", None),) + (P(),) * 5,
        out_specs=(tokens,) * 4 + (P("dp", None),),
        check_vma=False,
    )
```

time: 568 us -> 174 us (0.31)
  waiting for transfers between devices: 168 us -> 0 us
  Pallas kernels: 0 us -> 166 us
  local copies, waits for them, and re-layouts: 142 us -> 4.9 us
  other arithmetic: 91.2 us -> 0 us
  matrix products: 59.4 us -> 0 us
  starting transfers between devices: 57.9 us -> 0 us
  blocking collectives: 27.5 us -> 0 us
  between operations: 15.4 us -> 0.67 us
    pallas_call x0 -> x6, Pallas kernels: none -> 166 us  [the longest x1 70.8 us: chain(): pl.pallas_call(functools.partial(chain_kernel, n_sp), out_shape=(shape, s...]
    reduce_scatter x1 -> x0, waiting for transfers between devices: 79.8 us -> none  [per_device(): lax.psum_scatter(lax.dot_general(token_rows, pair_total, (((0,), (0,)), (...]
    all_gather x1 -> x0, waiting for transfers between devices: 59.7 us -> none  [over_pieces(): blocks = lax.all_gather(x, axis).astype(jnp.float32)]
    dot_general x18 -> x0, matrix products: 59.4 us -> none  [the longest x3 14.5 us: scan_heads(): local_out = jnp.einsum('clsh,cshp->clhp', mixing, scaled, precision=exact)]
    all_to_all x6 -> x0, starting transfers between devices: 57.8 us -> none  [the longest x2 16.6 us: in_one_piece(): lax.all_to_all(both, axis, split_axis=split_dim, concat_axis=concat_dim,...]
    unnamed x3 -> x0, other arithmetic: 49.8 us -> none
    unnamed x120 -> x5, local copies, waits for them, and re-layouts: 35.7 us -> 3.49 us
    broadcast_in_dim x4 -> x1, local copies, waits for them, and re-layouts: 32.3 us -> 0.73 us  [per_device(): skips = jnp.repeat(skip, HEAD).reshape(1, HEADS * HEAD)]
  transfers between devices with their start and end apart: 8 -> 0, of which waited for: 5 -> 0; matrix products, arithmetic and copies ran while one was open for 34% -> 0% of each run, Pallas kernels for 0% -> 0%
where the time goes in v1:
time: 174 us; the launch traced here: 172 us
  Pallas kernels  166 us (95%)
  local copies, waits for them, and re-layouts  4.9 us (3%)
    pallas_call x1, Pallas kernels, chain(): pl.pallas_call(functools.partial(chain_kernel, n_sp), out_shape=(shape, s...  70.8 us
    pallas_call x1, Pallas kernels, reduce(): pl.pallas_call(functools.partial(reduce_kernel, chips, n_sp), out_shape=(...  39.2 us
    pallas_call x1, Pallas kernels, gather(): pl.pallas_call(functools.partial(gather_kernel, chips, n_sp), out_shape=(...  29.4 us
    pallas_call x1, Pallas kernels, local(): pl.pallas_call(local_kernel, out_shape=(s((TOK, 512), f32), s((TOK, 512),...  12.5 us
    pallas_call x1, Pallas kernels, grads(): pl.pallas_call(grads_kernel, out_shape=(s((1, TOK, width), bf16), s((1, T...  11.1 us
    unnamed x5, local copies, waits for them, and re-layouts  3.49 us

profile of v1, /device:TPU:6, one launch (start us, length us, event | category | flops | bytes accessed | tf_op | source)
XLA Modules:
  0.0 171.9 jit_solution(3259935719426182292)
XLA Ops:
  0.6 0.7 broadcast_in_dim.3
  1.4 0.7 reshape_reshape.3.skips
  2.0 1.4 copy.18.raw
  3.4 29.4 %gather.1 = (bf16[16,2,64,512]{3,2,1,0:T(8,128)(2,1)}, bf16[2,16,2048]{2,1,0:T(8,128)(2,1)}) custom-call(bf16[64,512]{1,0:T(8,128)(2,1)} %proj.1, bf16[1,128,2048]{2,1,0:T(8,128)(2,1)} %values.5, bf16[1,128,2048]{2,1,0:T(8,128)(2,1)} %normed.5), custom_call_target="tpu_custom_call" | custom-call | tf_op jit(solution)/shard_map/gather/pallas_call | solution.py:83
  32.9 12.5 %local.1 = (f32[128,512]{1,0:T(8,128)}, f32[128,512]{1,0:T(8,128)}, f32[2048,128]{1,0:T(8,128)}, f32[2048,128]{1,0:T(8,128)}, f32[32,128]{1,0:T(8,128)}, /*index...) custom-call(s32[1]{0:T(128)} %bitcast.1.z_ref, bf16[2048,512]{1,0:T(8,128)(2,1)} %bitcast.4, ...), custom_call_target="tpu_custom_call" | custom-call | tf_op jit(solution)/shard_map/local/pallas_call | solution.py:202
  45.3 70.8 %chain.1 = (bf16[2048,128]{1,0:T(8,128)(2,1)}, bf16[2048,128]{1,0:T(8,128)(2,1)}) custom-call(f32[2048,128]{1,0:T(8,128)} %get-tuple-element.35.left, f32[2048,128]{1,0:T(8,128)} %get-tuple-element.37.right, f32[32,128]{1,0:T(8,128)} %get-tuple-element.36.dec), custom_call_target="tpu_custom_call" | custom-call | tf_op jit(solution)/shard_map/chain/pallas_call | solution.py:287
  116.1 11.1 %grads.1 = (bf16[1,128,2048]{2,1,0:T(8,128)(2,1)}, bf16[1,128,2048]{2,1,0:T(8,128)(2,1)}, bf16[1,128,32]{2,1,0:T(8,128)(2,1)}, f32[16,2048]{1,0:T(8,128)}, f32[1...) custom-call(s32[1]{0:T(128)} %bitcast.1.z_ref, ...), custom_call_target="tpu_custom_call" | custom-call | tf_op jit(solution)/shard_map/grads/pallas_call | solution.py:393
  127.3 1.4 copy.19
  128.7 39.2 %reduce.1 = (f32[64,512]{1,0:T(8,128)}, f32[16,2048]{1,0:T(8,128)}, f32[16,512]{1,0:T(8,128)}) custom-call(bf16[1,128,2048]{2,1,0:T(8,128)(2,1)} %normed.5, bf16[2,16,2048]{2,1,0:T(8,128)(2,1)} %get-tuple-element.32.halo, bf16[128,512]{1,0:T(8,128)(2,1)} %get-tuple-element.43.dp, bf16[16,512]{1,0:T(8,128)(2,1)} %get-tuple-element.45.dp_halo, ...), custom_call_target="tpu_custom_call" | custom-call | tf_op jit(solution)/shard_map/reduce/pallas_call | solution.py:485
  167.9 0.0 copy-start
  167.9 3.3 %finish.1 = (bf16[1,128,2048]{2,1,0:T(8,128)(2,1)}, bf16[1,128,2048]{2,1,0:T(8,128)(2,1)}) custom-call(bf16[2048,512]{1,0:T(8,128)(2,1)} %bitcast.5, bf16[128,512]{1,0:T(8,128)(2,1)} %get-tuple-element.43.dp, f32[16,512]{1,0:T(8,128)} %get-tuple-element.44.dp_tail, f32[16,512]{1,0:T(8,128)} %get-tuple-element.48.dp_after, ...), custom_call_target="tpu_custom_call", output_to_operand_aliasing={{1}: (6, {})} | custom-call | tf_op jit(solution)/shard_map/finish/pallas_call | solution.py:514
  171.2 0.0 copy-done
  171.2 0.7 copy.22
Async XLA Ops:
  167.9 3.4 %copy-start = (f32[64,512]{1,0:T(8,128)S(1)}, f32[64,512]{1,0:T(8,128)}, u32[]{:S(2)}) copy-start(f32[64,512]{1,0:T(8,128)} %get-tuple-element.71) | copy-start | bytes 393220
